TPU v7x, 32 devices: a whole 2x2x4 slice. The times are simulated.
32 devices in a mesh: sp: 8 (over z, y), dp: 4 (over x, core).
Axes of the slice: x: 2, y: 2, z: 4, core: 2. Of those that a mesh axis runs over, the one named last changes fastest.
Arguments:
- tokens: bfloat16 [4, 512, 1024], P('dp', 'sp'), may hold values from -6 to 6
- w_query: bfloat16 [1024, 512], P(None, ('sp', 'dp')), may hold values from -0.1875 to 0.1875
- w_forward: bfloat16 [1024, 512], P(None, ('sp', 'dp')), may hold values from -0.1875 to 0.1875
- w_backward: bfloat16 [1024, 512], P(None, ('sp', 'dp')), may hold values from -0.1875 to 0.1875
- w_input: bfloat16 [1024, 512], P(None, ('sp', 'dp')), may hold values from -0.1875 to 0.1875
- w_gate: bfloat16 [1024, 512], P(None, ('sp', 'dp')), may hold values from -0.1875 to 0.1875
- w_out: bfloat16 [512, 1024], P(None, ('sp', 'dp')), may hold values from -0.25 to 0.25
- memory_forward: float32 [512], replicated, may hold values from 0.3 to 4
- memory_backward: float32 [512], replicated, may hold values from 0.3 to 4
- norm_gain: float32 [128], replicated, may hold values from 0.1 to 1.9
Outputs:
- mixed: bfloat16 [4, 512, 1024], P('dp', 'sp')
All inputs are finite; a program needn't handle non-finite values.
Results may differ from a plain program's by a relative error of at most 0.015.
Values may be sent and summed in bfloat16 or wider, within the bound.
A program may use at most 64 MiB of HBM per device.

v0:
```python
import jax
import jax.numpy as jnp
from jax import lax
from jax.sharding import PartitionSpec as P

HEADS = 4
HEAD_DIM = 128
BLOCK = 64
norm_eps = 1e-06
highest = lax.Precision.HIGHEST


def as_sent(array):
    return jax.tree.map(lambda a: a.astype(jnp.bfloat16) if a.dtype == jnp.float32 else a, array)


def gathered_then(share, axis, dim, apply):
    everything = lax.all_gather(share, axis, axis=dim, tiled=True)
    return apply(everything, jnp.int32(0))


def log_forget(projected, memory, seq_len):
    slack_value = memory / seq_len
    return jnp.logaddexp(
        jnp.log1p(-slack_value),
        jnp.log(slack_value) + jax.nn.log_sigmoid(projected.astype(jnp.float32)),
    )


def sweep(queries, log_decay, values):
    seq_len, key_width = queries.shape
    blocks = seq_len // BLOCK
    input_keys = -jnp.expm1(log_decay)
    lower_mask = jnp.tril(jnp.ones((BLOCK, BLOCK), dtype=bool))[:, :, None]

    def advance(carry_state, inputs):
        query_part, decay_part, key_part, value_part = inputs
        running = jnp.cumsum(decay_part, axis=0)
        from_state = jnp.dot(query_part * jnp.exp(running), carry_state, precision=highest)
        gaps = running[:, None, :] - running[None, :, :]
        decay_table = jnp.where(lower_mask, jnp.exp(jnp.where(lower_mask, gaps, 0.0)), 0.0)
        scores = jnp.sum(query_part[:, None, :] * key_part[None, :, :] * decay_table, axis=2)
        inside = jnp.dot(scores, value_part, precision=highest)
        final_sum = running[-1]
        weighted = key_part * jnp.exp(final_sum[None, :] - running)
        carry_state = jnp.exp(final_sum)[:, None] * carry_state + jnp.dot(
            weighted.T, value_part, precision=highest
        )
        return (carry_state, from_state + inside)

    def blocked(array):
        return array.reshape(blocks, BLOCK, array.shape[1])

    zero_state = jnp.zeros((key_width, values.shape[1]), jnp.float32)
    _, readings = lax.scan(
        advance,
        zero_state,
        (blocked(queries), blocked(log_decay), blocked(input_keys), blocked(values)),
    )
    return readings.reshape(seq_len, values.shape[1])


def both_ways(queries, log_ahead, log_behind, values):
    forward_read = sweep(queries, log_ahead, values)
    behind = sweep(jnp.flip(queries, 0), jnp.flip(log_behind, 0), jnp.flip(values, 0))
    return forward_read + jnp.flip(behind, 0)


def body(
    tokens,
    w_query,
    w_forward,
    w_backward,
    w_input,
    w_gate,
    w_out,
    memory_forward,
    memory_backward,
    norm_gain,
):
    seq_count, tok_count, model_width = tokens.shape
    row_count = seq_count * tok_count
    flat_tokens = tokens.reshape(row_count, model_width)
    group_count = lax.axis_size("sp")
    per_head_groups = group_count // HEADS
    block_width = HEAD_DIM // per_head_groups
    head_index = lax.axis_index("sp") // per_head_groups
    full_query, full_forward, full_backward, full_input, full_gate = (
        lax.all_gather(w_query, ("sp", "dp"), axis=1, tiled=True),
        lax.all_gather(w_forward, ("sp", "dp"), axis=1, tiled=True),
        lax.all_gather(w_backward, ("sp", "dp"), axis=1, tiled=True),
        lax.all_gather(w_input, ("sp", "dp"), axis=1, tiled=True),
        lax.all_gather(w_gate, ("sp", "dp"), axis=1, tiled=True),
    )

    def project(weight):
        return jnp.dot(flat_tokens, weight, preferred_element_type=jnp.float32).astype(jnp.bfloat16)

    def by_head(projected):
        shaped = projected.reshape(row_count, HEADS, 1, HEAD_DIM)
        spread_out = jnp.broadcast_to(shaped, (row_count, HEADS, per_head_groups, HEAD_DIM))
        return spread_out.reshape(row_count, group_count, HEAD_DIM)

    def by_group(projected):
        return projected.reshape(row_count, group_count, block_width)

    query_heads, ahead_heads, behind_heads, value_heads = (
        lax.all_to_all(
            as_sent(by_head(project(full_query))), "sp", split_axis=1, concat_axis=0, tiled=True
        ),
        lax.all_to_all(
            as_sent(by_head(project(full_forward))), "sp", split_axis=1, concat_axis=0, tiled=True
        ),
        lax.all_to_all(
            as_sent(by_head(project(full_backward))), "sp", split_axis=1, concat_axis=0, tiled=True
        ),
        lax.all_to_all(
            as_sent(by_group(project(full_input))), "sp", split_axis=1, concat_axis=0, tiled=True
        ),
    )
    gate_rows = project(full_gate)
    seq_len = query_heads.shape[0]
    memory_ahead = lax.dynamic_slice_in_dim(memory_forward, head_index * HEAD_DIM, HEAD_DIM)
    memory_behind = lax.dynamic_slice_in_dim(memory_backward, head_index * HEAD_DIM, HEAD_DIM)
    queries = jax.nn.silu(query_heads[:, 0].astype(jnp.float32))
    log_ahead = log_forget(ahead_heads[:, 0], memory_ahead, seq_len)
    log_behind = log_forget(behind_heads[:, 0], memory_behind, seq_len)
    values = value_heads[:, 0].astype(jnp.float32)
    readout = both_ways(queries, log_ahead, log_behind, values).astype(jnp.bfloat16)
    returned = lax.all_to_all(
        readout.reshape(seq_len, 1, block_width), "sp", split_axis=0, concat_axis=1, tiled=True
    )
    readout_rows = returned.reshape(row_count, HEADS, HEAD_DIM).astype(jnp.float32)
    normed = (
        readout_rows
        * lax.rsqrt(jnp.mean(readout_rows * readout_rows, axis=-1, keepdims=True) + norm_eps)
        * norm_gain
    )
    normed = normed.reshape(row_count, HEADS * HEAD_DIM)
    gated_rows = (normed * jax.nn.silu(gate_rows.astype(jnp.float32))).astype(jnp.bfloat16)

    def output_block(weight_piece, first_index):
        return jnp.dot(gated_rows, weight_piece, preferred_element_type=jnp.float32).astype(
            jnp.bfloat16
        )

    mixed_rows = gathered_then(w_out, ("sp", "dp"), 1, output_block)
    return mixed_rows.reshape(seq_count, tok_count, model_width)


def solution(mesh):
    return jax.shard_map(
        body,
        mesh=mesh,
        in_specs=(
            P("dp", "sp", None),
            P(None, ("sp", "dp")),
            P(None, ("sp", "dp")),
            P(None, ("sp", "dp")),
            P(None, ("sp", "dp")),
            P(None, ("sp", "dp")),
            P(None, ("sp", "dp")),
            P(),
            P(),
            P(),
        ),
        out_specs=P("dp", "sp", None),
        check_vma=False,
    )
```

profile of v0, /device:TPU:0, one launch (start us, length us, event | category | flops | bytes accessed | tf_op | source)
XLA Modules:
  0.0 354.7 jit_solution(13744162278260831660)
XLA Ops:
  12.1 54.5 %all-gather.13.cloned.1.call-done = bf16[1024,512]{0,1:T(8,128)(2,1)} async-done(((bf16[1024,16]{0,1:T(8,128)(2,1)}), bf16[1024,512]{0,1:T(8,128)(2,1)}) %all-gather.13.cloned.1.call-update) | async-done | bytes 1048592 | tf_op jit(solution)/shard_map/all_gather | solution.py:91
  66.6 1.7 fusion.54
  68.2 53.8 %all-gather.9.cloned.1.call-done = bf16[1024,512]{0,1:T(8,128)(2,1)} async-done(((bf16[1024,16]{0,1:T(8,128)(2,1)}), bf16[1024,512]{0,1:T(8,128)(2,1)}) %all-gather.9.cloned.1.call-update) | async-done | bytes 1048592 | tf_op jit(solution)/shard_map/all_gather | solution.py:92
  122.0 1.7 convolution_convert_fusion.4
  124.7 4.5 %all-to-all-start.1 = ((bf16[8,2,2048]{2,1,0:T(2,128)(2,1)}), bf16[8,2,2048]{2,1,0:T(2,128)(2,1)S(1)}, u32[]{:S(2)}, u32[]{:S(2)}) async-start(bf16[8,2,2048]{2,1,0:T(2,128)(2,1)} %reshape.264), calls=%async_computation.1 | async-start | bytes 131072 | tf_op jit(solution)/shard_map/all_to_all | solution.py:117
  129.2 48.4 %all-gather.11.cloned.1.call-done = bf16[1024,512]{0,1:T(8,128)(2,1)} async-done(((bf16[1024,16]{0,1:T(8,128)(2,1)}), bf16[1024,512]{0,1:T(8,128)(2,1)}) %all-gather.11.cloned.1.call-update) | async-done | bytes 1048592 | tf_op jit(solution)/shard_map/all_gather | solution.py:89
  177.5 1.7 fusion.53
  179.2 53.6 %all-gather.7.cloned.1.call-done = bf16[1024,512]{0,1:T(8,128)(2,1)} async-done(((bf16[1024,16]{0,1:T(8,128)(2,1)}), bf16[1024,512]{0,1:T(8,128)(2,1)}) %all-gather.7.cloned.1.call-update) | async-done | bytes 1048592 | tf_op jit(solution)/shard_map/all_gather | solution.py:90
  232.9 1.7 fusion.52
  235.2 4.5 %all-to-all-start.3 = ((bf16[64,8,128]{2,0,1:T(8,128)(2,1)}), bf16[64,8,128]{2,0,1:T(8,128)(2,1)S(1)}, u32[]{:S(2)}, u32[]{:S(2)}) async-start(bf16[64,8,128]{2,0,1:T(8,128)(2,1)} %bitcast.17), calls=%async_computation.3 | async-start | bytes 262144 | tf_op jit(solution)/shard_map/all_to_all | solution.py:114
  240.1 7.1 %all-to-all-done.3 = bf16[64,8,128]{2,0,1:T(8,128)(2,1)S(1)} async-done(((bf16[64,8,128]{2,0,1:T(8,128)(2,1)}), bf16[64,8,128]{2,0,1:T(8,128)(2,1)S(1)}, u32[]{:S(2)}, u32[]{:S(2)}) %all-to-all-start.3) | async-done | bytes 131104 | tf_op jit(solution)/shard_map/all_to_all | solution.py:114
  247.8 3.4 all-to-all-start.2
  251.8 6.7 %all-to-all-done.2 = bf16[64,8,128]{2,0,1:T(8,128)(2,1)S(1)} async-done(((bf16[64,8,128]{2,0,1:T(8,128)(2,1)}), bf16[64,8,128]{2,0,1:T(8,128)(2,1)S(1)}, u32[]{:S(2)}, u32[]{:S(2)}) %all-to-all-start.2) | async-done | bytes 131104 | tf_op jit(solution)/shard_map/all_to_all | solution.py:108
  259.1 3.4 all-to-all-start
  262.8 17.5 %while.29 = (s32[]{:T(128)}, f32[128,64]{0,1:T(8,128)S(1)}, f32[8,64,64]{2,1,0:T(8,128)S(1)}, f32[8,64,128]{2,1,0:T(8,128)S(1)}, f32[8,64,128]{2,1,0:T(8,128)S(1...) while((s32[]{:T(128)}, f32[128,64]{0,1:T(8,128)S(1)}, ...), condition=%wide.region_7.8_spmd.clone.clone, body=%wide.region_4.7_spmd.clone.clone.sunk | while | flops 19451908 | bytes 799868 | solution.py:55
  262.9 1.4 multiply_reduce_fusion.6
  271.6 1.4 multiply_reduce_fusion.6
  280.8 17.5 %while.28 = (s32[]{:T(128)}, f32[128,64]{0,1:T(8,128)S(1)}, f32[8,64,64]{2,1,0:T(8,128)S(1)}, f32[8,64,128]{2,1,0:T(8,128)S(1)}, f32[8,64,128]{2,1,0:T(8,128)S(1...) while((s32[]{:T(128)}, f32[128,64]{0,1:T(8,128)S(1)}, ...), condition=%wide.region_3.4_spmd.clone.clone, body=%wide.region_0.3_spmd.clone.clone.sunk | while | flops 19451908 | bytes 799868 | solution.py:55
  280.9 1.4 multiply_reduce_fusion.5
  294.0 1.4 multiply_reduce_fusion.5
  301.0 5.9 %all-to-all-start.4 = ((bf16[8,2,2048]{2,1,0:T(2,128)(2,1)}), bf16[8,2,2048]{2,1,0:T(2,128)(2,1)S(1)}, u32[]{:S(2)}, u32[]{:S(2)}) async-start(bf16[8,2,2048]{2,1,0:T(2,128)(2,1)} %reshape.266), calls=%async_computation.4 | async-start | bytes 131072 | tf_op jit(solution)/shard_map/all_to_all | solution.py:130
  306.9 6.9 %all-to-all-done.4 = bf16[8,2,2048]{2,1,0:T(2,128)(2,1)S(1)} async-done(((bf16[8,2,2048]{2,1,0:T(2,128)(2,1)}), bf16[8,2,2048]{2,1,0:T(2,128)(2,1)S(1)}, u32[]{:S(2)}, u32[]{:S(2)}) %all-to-all-start.4) | async-done | bytes 65568 | tf_op jit(solution)/shard_map/all_to_all | solution.py:130
  314.7 29.9 %all-gather.17.cloned.1.call-done = bf16[512,1024]{0,1:T(8,128)(2,1)} async-done(((bf16[512,32]{0,1:T(8,128)(2,1)}), bf16[512,1024]{0,1:T(8,128)(2,1)}) %all-gather.17.cloned.1.call-update) | async-done | bytes 1048592 | tf_op jit(solution)/shard_map/all_gather | solution.py:18
  344.8 3.0 fusion.50
  (221 shorter events, 41.8 us)
Async XLA Ops:
  6.5 60.0 %copy-start = (bf16[1,64,1024]{2,1,0:T(8,128)(2,1)S(1)}, bf16[1,64,1024]{2,1,0:T(8,128)(2,1)}, u32[]{:S(2)}) copy-start(bf16[1,64,1024]{2,1,0:T(8,128)(2,1)} %param.14) | copy-start | bytes 393220
  6.5 60.0 %all-gather.13.cloned.1.call-start = ((), (), s32[]{:S(2)}) async-start(), calls=%async_computation.8 | async-start | bytes 1081344 | tf_op jit(solution)/shard_map/all_gather | solution.py:91
  7.3 114.8 %all-gather.9.cloned.1.call-start = ((), (), s32[]{:S(2)}) async-start(), calls=%async_computation.6 | async-start | bytes 1081344 | tf_op jit(solution)/shard_map/all_gather | solution.py:92
  8.0 169.5 %all-gather.11.cloned.1.call-start = ((), (), s32[]{:S(2)}) async-start(), calls=%async_computation.7 | async-start | bytes 1081344 | tf_op jit(solution)/shard_map/all_gather | solution.py:89
  8.7 224.1 %all-gather.7.cloned.1.call-start = ((), (), s32[]{:S(2)}) async-start(), calls=%async_computation.5 | async-start | bytes 1081344 | tf_op jit(solution)/shard_map/all_gather | solution.py:90
  9.3 305.4 %all-gather.15.cloned.1.call-start = ((), (), s32[]{:S(2)}) async-start(), calls=%async_computation.9 | async-start | bytes 1081344 | tf_op jit(solution)/shard_map/all_gather | solution.py:93
  9.9 334.8 %all-gather.17.cloned.1.call-start = ((), (), s32[]{:S(2)}) async-start(), calls=%async_computation.10 | async-start | bytes 1081344 | tf_op jit(solution)/shard_map/all_gather | solution.py:18
  124.7 109.9 %all-to-all-start.1 = ((bf16[8,2,2048]{2,1,0:T(2,128)(2,1)}), bf16[8,2,2048]{2,1,0:T(2,128)(2,1)S(1)}, u32[]{:S(2)}, u32[]{:S(2)}) async-start(bf16[8,2,2048]{2,1,0:T(2,128)(2,1)} %reshape.264), calls=%async_computation.1 | async-start | bytes 131072 | tf_op jit(solution)/shard_map/all_to_all | solution.py:117
  235.2 11.9 %all-to-all-start.3 = ((bf16[64,8,128]{2,0,1:T(8,128)(2,1)}), bf16[64,8,128]{2,0,1:T(8,128)(2,1)S(1)}, u32[]{:S(2)}, u32[]{:S(2)}) async-start(bf16[64,8,128]{2,0,1:T(8,128)(2,1)} %bitcast.17), calls=%async_computation.3 | async-start | bytes 262144 | tf_op jit(solution)/shard_map/all_to_all | solution.py:114
  247.8 10.7 %all-to-all-start.2 = ((bf16[64,8,128]{2,0,1:T(8,128)(2,1)}), bf16[64,8,128]{2,0,1:T(8,128)(2,1)S(1)}, u32[]{:S(2)}, u32[]{:S(2)}) async-start(bf16[64,8,128]{2,0,1:T(8,128)(2,1)} %bitcast.10), calls=%async_computation.2 | async-start | bytes 262144 | tf_op jit(solution)/shard_map/all_to_all | solution.py:108
  259.1 21.2 %all-to-all-start = ((bf16[64,8,128]{2,0,1:T(8,128)(2,1)}), bf16[64,8,128]{2,0,1:T(8,128)(2,1)S(1)}, u32[]{:S(2)}, u32[]{:S(2)}) async-start(bf16[64,8,128]{2,0,1:T(8,128)(2,1)} %bitcast.1), calls=%async_computation | async-start | bytes 262144 | tf_op jit(solution)/shard_map/all_to_all | solution.py:111
  298.2 8.7 %copy-start.1 = (f32[128]{0:T(128)S(1)}, f32[128]{0:T(128)}, u32[]{:S(2)}) copy-start(f32[128]{0:T(128)} %param.23) | copy-start | bytes 1540
  301.0 12.8 %all-to-all-start.4 = ((bf16[8,2,2048]{2,1,0:T(2,128)(2,1)}), bf16[8,2,2048]{2,1,0:T(2,128)(2,1)S(1)}, u32[]{:S(2)}, u32[]{:S(2)}) async-start(bf16[8,2,2048]{2,1,0:T(2,128)(2,1)} %reshape.266), calls=%async_computation.4 | async-start | bytes 131072 | tf_op jit(solution)/shard_map/all_to_all | solution.py:130
Sparse Core Ops, SparseCore 0:
  10.2 56.3 all-gather.12
  69.4 52.5 all-gather.8
  124.9 52.5 all-gather.10
  180.2 52.5 all-gather.6
  235.6 53.3 all-gather.14
  291.7 52.8 all-gather.16
where the time goes:
time: 355 us
  waiting for transfers between devices  265 us (75%)
  other arithmetic  26.9 us (8%)
  starting transfers between devices  21.8 us (6%)
  matrix products  19.3 us (5%)
  between operations  13.8 us (4%)
  local copies, waits for them, and re-layouts  6.91 us (2%)
    all_gather x1, waiting for transfers between devices, body(): lax.all_gather(w_backward, ('sp', 'dp'), axis=1, tiled=True)  54.5 us
    all_gather x1, waiting for transfers between devices, body(): lax.all_gather(w_input, ('sp', 'dp'), axis=1, tiled=True)  53.8 us
    all_gather x1, waiting for transfers between devices, body(): lax.all_gather(w_forward, ('sp', 'dp'), axis=1, tiled=True)  53.6 us
    all_gather x1, waiting for transfers between devices, body(): lax.all_gather(w_query, ('sp', 'dp'), axis=1, tiled=True)  48.4 us
    all_gather x1, waiting for transfers between devices, gathered_then(): everything = lax.all_gather(share, axis, axis=dim, tiled=True)  29.9 us
    reduce_sum x16, other arithmetic, advance(): jnp.sum(query_part[:, None, :] * key_part[None, :, :] * decay_table, axis=2)  21.8 us
  transfers between devices with their start and end apart: 11, of which 8 were waited for; matrix products, arithmetic and copies ran while one was open for 14% of the time, Pallas kernels for 0%

commit v1 on v0

--- a/solution.py
+++ b/solution.py
@@ -86,7 +86,10 @@
     block_width = HEAD_DIM // per_head_groups
     head_index = lax.axis_index("sp") // per_head_groups
     full_query, full_forward, full_backward, full_input, full_gate = (
-        lax.all_gather(w_query, ("sp", "dp"), axis=1, tiled=True),
+        jnp.concatenate(
+            lax.all_to_all(jnp.stack([w_query] * lax.axis_size(("sp", "dp"))), ("sp", "dp"), 0, 0),
+            axis=1,
+        ),
         lax.all_gather(w_forward, ("sp", "dp"), axis=1, tiled=True),
         lax.all_gather(w_backward, ("sp", "dp"), axis=1, tiled=True),
         lax.all_gather(w_input, ("sp", "dp"), axis=1, tiled=True),

time: 355 us -> 302 us (0.85)
  waiting for transfers between devices: 265 us -> 207 us
  starting transfers between devices: 21.8 us -> 25.5 us
    all_gather x1 -> x0, waiting for transfers between devices: 48.4 us -> none  [body(): lax.all_gather(w_query, ('sp', 'dp'), axis=1, tiled=True)]
    all_gather x1, waiting for transfers between devices: 29.9 us -> 14.8 us  [gathered_then(): everything = lax.all_gather(share, axis, axis=dim, tiled=True)]
    all_to_all x0 -> x1, starting transfers between devices: none -> 7.33 us  [body(): lax.all_to_all(jnp.stack([w_query] * lax.axis_size(('sp', 'dp'))), ('sp',...]
    all_to_all x1, waiting for transfers between devices: 0.01 us -> 7.11 us  [body(): lax.all_to_all(as_sent(by_head(project(full_forward))), 'sp', split_axis=...]
    all_to_all x1, waiting for transfers between devices: 0.01 us -> 6.44 us  [body(): lax.all_to_all(as_sent(by_group(project(full_input))), 'sp', split_axis=1...]
    all_gather x1, waiting for transfers between devices: 54.5 us -> 48.4 us  [body(): lax.all_gather(w_backward, ('sp', 'dp'), axis=1, tiled=True)]
  transfers between devices with their start and end apart: 11 -> 11, of which waited for: 8 -> 9; matrix products, arithmetic and copies ran while one was open for 14% -> 17% of each run, Pallas kernels for 0% -> 0%
where the time goes in v1:
time: 302 us; the launch traced here: 301 us
  waiting for transfers between devices  207 us (69%)
  other arithmetic  26.9 us (9%)
  starting transfers between devices  25.5 us (8%)
  matrix products  18.1 us (6%)
  between operations  13.5 us (4%)
  local copies, waits for them, and re-layouts  8.84 us (3%)
    all_gather x1, waiting for transfers between devices, body(): lax.all_gather(w_input, ('sp', 'dp'), axis=1, tiled=True)  53.8 us
    all_gather x1, waiting for transfers between devices, body(): lax.all_gather(w_forward, ('sp', 'dp'), axis=1, tiled=True)  52.9 us
    all_gather x1, waiting for transfers between devices, body(): lax.all_gather(w_backward, ('sp', 'dp'), axis=1, tiled=True)  48.4 us
    reduce_sum x16, other arithmetic, advance(): jnp.sum(query_part[:, None, :] * key_part[None, :, :] * decay_table, axis=2)  21.8 us
    all_gather x1, waiting for transfers between devices, gathered_then(): everything = lax.all_gather(share, axis, axis=dim, tiled=True)  14.8 us
    all_to_all x1, starting transfers between devices, body(): lax.all_to_all(jnp.stack([w_query] * lax.axis_size(('sp', 'dp'))), ('sp',...  7.33 us
    all_to_all x1, waiting for transfers between devices, body(): lax.all_to_all(as_sent(by_head(project(full_forward))), 'sp', split_axis=...  7.11 us
    all_to_all x1, waiting for transfers between devices, body(): lax.all_to_all(as_sent(by_head(project(full_backward))), 'sp', split_axis...  6.95 us
  transfers between devices with their start and end apart: 11, of which 9 were waited for; matrix products, arithmetic and copies ran while one was open for 17% of the time, Pallas kernels for 0%

profile of v1, /device:TPU:0, one launch (start us, length us, event | category | flops | bytes accessed | tf_op | source)
XLA Modules:
  0.0 301.4 jit_solution(14765545155925876553)
XLA Ops:
  9.3 1.9 stack.2
  11.2 7.3 %all-to-all-start.2 = ((bf16[32,1024,16]{1,2,0:T(8,128)(2,1)}), bf16[32,1024,16]{1,2,0:T(8,128)(2,1)S(1)}, u32[]{:S(2)}, u32[]{:S(2)}) async-start(bf16[32,1024,16]{1,2,0:T(8,128)(2,1)} %stack.2), calls=%async_computation.2 | async-start | bytes 2097152 | tf_op jit(solution)/shard_map/all_to_all | solution.py:90
  20.7 48.4 %all-gather.10.cloned.1.call-done = bf16[1024,512]{0,1:T(8,128)(2,1)} async-done(((bf16[1024,16]{0,1:T(8,128)(2,1)}), bf16[1024,512]{0,1:T(8,128)(2,1)}) %all-gather.10.cloned.1.call-update) | async-done | bytes 1048592 | tf_op jit(solution)/shard_map/all_gather | solution.py:94
  69.2 1.7 fusion.54
  70.8 53.8 %all-gather.8.cloned.1.call-done = bf16[1024,512]{0,1:T(8,128)(2,1)} async-done(((bf16[1024,16]{0,1:T(8,128)(2,1)}), bf16[1024,512]{0,1:T(8,128)(2,1)}) %all-gather.8.cloned.1.call-update) | async-done | bytes 1048592 | tf_op jit(solution)/shard_map/all_gather | solution.py:95
  124.6 1.7 convolution_convert_fusion.4
  127.2 52.9 %all-gather.6.cloned.1.call-done = bf16[1024,512]{0,1:T(8,128)(2,1)} async-done(((bf16[1024,16]{0,1:T(8,128)(2,1)}), bf16[1024,512]{0,1:T(8,128)(2,1)}) %all-gather.6.cloned.1.call-update) | async-done | bytes 1048592 | tf_op jit(solution)/shard_map/all_gather | solution.py:93
  180.1 1.7 fusion.52
  181.8 4.5 %all-to-all-start.1 = ((bf16[8,2,2048]{2,1,0:T(2,128)(2,1)}), bf16[8,2,2048]{2,1,0:T(2,128)(2,1)S(1)}, u32[]{:S(2)}, u32[]{:S(2)}) async-start(bf16[8,2,2048]{2,1,0:T(2,128)(2,1)} %reshape.274), calls=%async_computation.1 | async-start | bytes 131072 | tf_op jit(solution)/shard_map/all_to_all | solution.py:120
  186.8 6.4 %all-to-all-done.1 = bf16[8,2,2048]{2,1,0:T(2,128)(2,1)S(1)} async-done(((bf16[8,2,2048]{2,1,0:T(2,128)(2,1)}), bf16[8,2,2048]{2,1,0:T(2,128)(2,1)S(1)}, u32[]{:S(2)}, u32[]{:S(2)}) %all-to-all-start.1) | async-done | bytes 65568 | tf_op jit(solution)/shard_map/all_to_all | solution.py:120
  193.9 3.4 %all-to-all-start.4 = ((bf16[64,8,128]{2,0,1:T(8,128)(2,1)}), bf16[64,8,128]{2,0,1:T(8,128)(2,1)S(1)}, u32[]{:S(2)}, u32[]{:S(2)}) async-start(bf16[64,8,128]{2,0,1:T(8,128)(2,1)} %bitcast.19), calls=%async_computation.4 | async-start | bytes 262144 | tf_op jit(solution)/shard_map/all_to_all | solution.py:117
  197.6 6.9 %all-to-all-done.4 = bf16[64,8,128]{2,0,1:T(8,128)(2,1)S(1)} async-done(((bf16[64,8,128]{2,0,1:T(8,128)(2,1)}), bf16[64,8,128]{2,0,1:T(8,128)(2,1)S(1)}, u32[]{:S(2)}, u32[]{:S(2)}) %all-to-all-start.4) | async-done | bytes 131104 | tf_op jit(solution)/shard_map/all_to_all | solution.py:117
  205.2 3.4 %all-to-all-start = ((bf16[64,8,128]{2,0,1:T(8,128)(2,1)}), bf16[64,8,128]{2,0,1:T(8,128)(2,1)S(1)}, u32[]{:S(2)}, u32[]{:S(2)}) async-start(bf16[64,8,128]{2,0,1:T(8,128)(2,1)} %bitcast.1), calls=%async_computation | async-start | bytes 262144 | tf_op jit(solution)/shard_map/all_to_all | solution.py:114
  209.1 7.1 %all-to-all-done = bf16[64,8,128]{2,0,1:T(8,128)(2,1)S(1)} async-done(((bf16[64,8,128]{2,0,1:T(8,128)(2,1)}), bf16[64,8,128]{2,0,1:T(8,128)(2,1)S(1)}, u32[]{:S(2)}, u32[]{:S(2)}) %all-to-all-start) | async-done | bytes 131104 | tf_op jit(solution)/shard_map/all_to_all | solution.py:114
  216.9 3.4 %all-to-all-start.3 = ((bf16[64,8,128]{2,0,1:T(8,128)(2,1)}), bf16[64,8,128]{2,0,1:T(8,128)(2,1)S(1)}, u32[]{:S(2)}, u32[]{:S(2)}) async-start(bf16[64,8,128]{2,0,1:T(8,128)(2,1)} %bitcast.12), calls=%async_computation.3 | async-start | bytes 262144 | tf_op jit(solution)/shard_map/all_to_all | solution.py:111
  220.8 6.9 %all-to-all-done.3 = bf16[64,8,128]{2,0,1:T(8,128)(2,1)S(1)} async-done(((bf16[64,8,128]{2,0,1:T(8,128)(2,1)}), bf16[64,8,128]{2,0,1:T(8,128)(2,1)S(1)}, u32[]{:S(2)}, u32[]{:S(2)}) %all-to-all-start.3) | async-done | bytes 131104 | tf_op jit(solution)/shard_map/all_to_all | solution.py:111
  227.9 17.5 %while.29 = (s32[]{:T(128)}, f32[128,64]{0,1:T(8,128)S(1)}, f32[8,64,64]{2,1,0:T(8,128)S(1)}, f32[8,64,128]{2,1,0:T(8,128)S(1)}, f32[8,64,128]{2,1,0:T(8,128)S(1...) while((s32[]{:T(128)}, f32[128,64]{0,1:T(8,128)S(1)}, ...), condition=%wide.region_7.8_spmd.clone.clone, body=%wide.region_4.7_spmd.clone.clone.sunk | while | flops 19451908 | bytes 799868 | solution.py:55
  228.1 1.4 multiply_reduce_fusion.6
  241.2 1.4 multiply_reduce_fusion.6
  245.5 17.5 %while.28 = (s32[]{:T(128)}, f32[128,64]{0,1:T(8,128)S(1)}, f32[8,64,64]{2,1,0:T(8,128)S(1)}, f32[8,64,128]{2,1,0:T(8,128)S(1)}, f32[8,64,128]{2,1,0:T(8,128)S(1...) while((s32[]{:T(128)}, f32[128,64]{0,1:T(8,128)S(1)}, ...), condition=%wide.region_3.4_spmd.clone.clone, body=%wide.region_0.3_spmd.clone.clone.sunk | while | flops 19451908 | bytes 799868 | solution.py:55
  265.7 3.4 %all-to-all-start.5 = ((bf16[8,2,2048]{2,1,0:T(2,128)(2,1)}), bf16[8,2,2048]{2,1,0:T(2,128)(2,1)S(1)}, u32[]{:S(2)}, u32[]{:S(2)}) async-start(bf16[8,2,2048]{2,1,0:T(2,128)(2,1)} %reshape.276), calls=%async_computation.5 | async-start | bytes 131072 | tf_op jit(solution)/shard_map/all_to_all | solution.py:133
  269.1 6.8 %all-to-all-done.5 = bf16[8,2,2048]{2,1,0:T(2,128)(2,1)S(1)} async-done(((bf16[8,2,2048]{2,1,0:T(2,128)(2,1)}), bf16[8,2,2048]{2,1,0:T(2,128)(2,1)S(1)}, u32[]{:S(2)}, u32[]{:S(2)}) %all-to-all-start.5) | async-done | bytes 65568 | tf_op jit(solution)/shard_map/all_to_all | solution.py:133
  276.9 14.8 %all-gather.14.cloned.1.call-done = bf16[512,1024]{0,1:T(8,128)(2,1)} async-done(((bf16[512,32]{0,1:T(8,128)(2,1)}), bf16[512,1024]{0,1:T(8,128)(2,1)}) %all-gather.14.cloned.1.call-update) | async-done | bytes 1048592 | tf_op jit(solution)/shard_map/all_gather | solution.py:18
  291.8 3.0 %fusion.50 = bf16[1,64,1024]{2,1,0:T(8,128)(2,1)} fusion(bf16[512,1024]{0,1:T(8,128)(2,1)} %all-gather.14.cloned.1.call-done, f32[64,512]{1,0:T(8,128)S(1)} %reshape.268, f32[8,8,4,128]{3,2,1,0:T(4,128)S(1)} %bitcast.290, bf16[1024,512]{0,1:T(8,128)(2,1)} %all-gather.12.cloned.1.call-done, bf16[1,64,1024]{2,1,0:T(8,128)(2,1)S(1)} %copy-done, ...), kind=kOutput, calls=%fused_computation.65 | convolution fusion | flops 134610944 | bytes 2623488 | tf_op jit(solution)/shard_map/dot_general | solution.py:146
  (221 shorter events, 44.5 us)
Async XLA Ops:
  6.5 62.6 %copy-start = (bf16[1,64,1024]{2,1,0:T(8,128)(2,1)S(1)}, bf16[1,64,1024]{2,1,0:T(8,128)(2,1)}, u32[]{:S(2)}) copy-start(bf16[1,64,1024]{2,1,0:T(8,128)(2,1)} %param.14) | copy-start | bytes 393220
  6.5 62.6 %all-gather.10.cloned.1.call-start = ((), (), s32[]{:S(2)}) async-start(), calls=%async_computation.8 | async-start | bytes 1081344 | tf_op jit(solution)/shard_map/all_gather | solution.py:94
  7.3 117.4 %all-gather.8.cloned.1.call-start = ((), (), s32[]{:S(2)}) async-start(), calls=%async_computation.7 | async-start | bytes 1081344 | tf_op jit(solution)/shard_map/all_gather | solution.py:95
  8.0 172.1 %all-gather.6.cloned.1.call-start = ((), (), s32[]{:S(2)}) async-start(), calls=%async_computation.6 | async-start | bytes 1081344 | tf_op jit(solution)/shard_map/all_gather | solution.py:93
  8.7 268.1 %all-gather.12.cloned.1.call-start = ((), (), s32[]{:S(2)}) async-start(), calls=%async_computation.9 | async-start | bytes 1081344 | tf_op jit(solution)/shard_map/all_gather | solution.py:96
  11.2 170.6 %all-to-all-start.2 = ((bf16[32,1024,16]{1,2,0:T(8,128)(2,1)}), bf16[32,1024,16]{1,2,0:T(8,128)(2,1)S(1)}, u32[]{:S(2)}, u32[]{:S(2)}) async-start(bf16[32,1024,16]{1,2,0:T(8,128)(2,1)} %stack.2), calls=%async_computation.2 | async-start | bytes 2097152 | tf_op jit(solution)/shard_map/all_to_all | solution.py:90
  18.5 273.1 %all-gather.14.cloned.1.call-start = ((), (), s32[]{:S(2)}) async-start(), calls=%async_computation.10 | async-start | bytes 1081344 | tf_op jit(solution)/shard_map/all_gather | solution.py:18
  181.8 11.4 %all-to-all-start.1 = ((bf16[8,2,2048]{2,1,0:T(2,128)(2,1)}), bf16[8,2,2048]{2,1,0:T(2,128)(2,1)S(1)}, u32[]{:S(2)}, u32[]{:S(2)}) async-start(bf16[8,2,2048]{2,1,0:T(2,128)(2,1)} %reshape.274), calls=%async_computation.1 | async-start | bytes 131072 | tf_op jit(solution)/shard_map/all_to_all | solution.py:120
  193.9 10.7 %all-to-all-start.4 = ((bf16[64,8,128]{2,0,1:T(8,128)(2,1)}), bf16[64,8,128]{2,0,1:T(8,128)(2,1)S(1)}, u32[]{:S(2)}, u32[]{:S(2)}) async-start(bf16[64,8,128]{2,0,1:T(8,128)(2,1)} %bitcast.19), calls=%async_computation.4 | async-start | bytes 262144 | tf_op jit(solution)/shard_map/all_to_all | solution.py:117
  205.2 11.0 %all-to-all-start = ((bf16[64,8,128]{2,0,1:T(8,128)(2,1)}), bf16[64,8,128]{2,0,1:T(8,128)(2,1)S(1)}, u32[]{:S(2)}, u32[]{:S(2)}) async-start(bf16[64,8,128]{2,0,1:T(8,128)(2,1)} %bitcast.1), calls=%async_computation | async-start | bytes 262144 | tf_op jit(solution)/shard_map/all_to_all | solution.py:114
  216.9 10.8 %all-to-all-start.3 = ((bf16[64,8,128]{2,0,1:T(8,128)(2,1)}), bf16[64,8,128]{2,0,1:T(8,128)(2,1)S(1)}, u32[]{:S(2)}, u32[]{:S(2)}) async-start(bf16[64,8,128]{2,0,1:T(8,128)(2,1)} %bitcast.12), calls=%async_computation.3 | async-start | bytes 262144 | tf_op jit(solution)/shard_map/all_to_all | solution.py:111
  263.0 6.1 %copy-start.1 = (f32[128]{0:T(128)S(1)}, f32[128]{0:T(128)}, u32[]{:S(2)}) copy-start(f32[128]{0:T(128)} %param.23) | copy-start | bytes 1540
  265.7 10.2 %all-to-all-start.5 = ((bf16[8,2,2048]{2,1,0:T(2,128)(2,1)}), bf16[8,2,2048]{2,1,0:T(2,128)(2,1)S(1)}, u32[]{:S(2)}, u32[]{:S(2)}) async-start(bf16[8,2,2048]{2,1,0:T(2,128)(2,1)} %reshape.276), calls=%async_computation.5 | async-start | bytes 131072 | tf_op jit(solution)/shard_map/all_to_all | solution.py:133
Sparse Core Ops, SparseCore 0:
  10.2 58.9 all-gather.9
  72.0 52.5 all-gather.7
  127.5 52.5 all-gather.5
  182.8 52.9 all-gather.11
  238.6 53.0 all-gather.13
